TPU v7x, 32 devices: a whole 2x2x4 slice. The times are simulated.
32 devices in a mesh: ep: 8 (over z, y), tp: 4 (over x, core).
Axes of the slice: x: 2, y: 2, z: 4, core: 2. Of those that a mesh axis runs over, the one named last changes fastest.
Arguments:
- queries_a: bfloat16 [1024, 1024], P('ep', 'tp'), may hold values from -128 to 128
- queries_b: bfloat16 [1024, 1024], P('ep', 'tp'), may hold values from -128 to 128
- keys_a: bfloat16 [1024, 512], P('ep', 'tp'), may hold values from -8 to 8
- keys_b: bfloat16 [1024, 512], P('ep', 'tp'), may hold values from -8 to 8
- values: bfloat16 [1024, 1024], P('ep', 'tp'), may hold values from -6 to 6
- lambdas: float32 [16], P('tp'), may hold values from 0.3 to 0.8
- head_gain: float32 [128], replicated, may hold values from 0.1 to 1.9
- w_out: bfloat16 [2048, 2048], P('tp'), may hold values from -0.125 to 0.125
- moe_tokens: bfloat16 [4096, 2048], P(('ep', 'tp')), may hold values from -80 to 80
- moe_gain: float32 [2048], replicated, may hold values from 0.1 to 1.9
- routes: int32 [4096, 2], P(('ep', 'tp')), may hold values from 0 to 7, all different within a row; in each aligned block of 128 rows (0 to 127, 128 to 255, ...) at most 48 rows name the same one
- route_weights: float32 [4096, 2], P(('ep', 'tp')), may hold values from 0.1 to 1
- w_gate: bfloat16 [8, 2048, 2048], P('ep', None, 'tp'), may hold values from -4 to 4
- w_up: bfloat16 [8, 2048, 2048], P('ep', None, 'tp'), may hold values from -4 to 4
- w_down: bfloat16 [8, 2048, 2048], P('ep', 'tp'), may hold values from -0.0625 to 0.0625
Outputs:
- mixer_out: bfloat16 [1024, 2048], P(('ep', 'tp'))
- moe_out: bfloat16 [4096, 2048], P(('ep', 'tp'))
Inputs may be any that keep to these rules, and one draw needn't show every extreme that they name: `routes`: each row names 2 different experts. Within the rows of one device no expert is named by more than 48 rows, a bound that some block reaches of some device.
All inputs are finite; a program needn't handle non-finite values.
Results may differ from a plain program's by a relative error of at most 0.011.
Values may be sent and summed in bfloat16 or wider, within the bound.
A program may use at most 192 MiB of HBM per device.

v0:
```python
import jax
import jax.numpy as jnp
from jax import lax
from jax.sharding import PartitionSpec as P

HEAD = 64
VDIM = 128
TOP = 2


eps = 1e-05
alpha_act = 1.702
limit_act = 7.0
negative = -1e30


def clamped_unit(gate, up):
    capped = jnp.minimum(gate, limit_act)
    linear = jnp.clip(up, -limit_act, limit_act)
    return capped * jax.nn.sigmoid(alpha_act * capped) * (linear + 1.0)


def hidden_rows(inputs, gate_matrix, up_matrix):
    gate = jnp.dot(inputs, gate_matrix, preferred_element_type=jnp.float32)
    up = jnp.dot(inputs, up_matrix, preferred_element_type=jnp.float32)
    return clamped_unit(gate, up).astype(jnp.bfloat16)


def pick_rows(table, owner):
    valid = owner < table.shape[0]
    chosen = jnp.take(table, jnp.minimum(owner, table.shape[0] - 1), axis=0)
    return jnp.where(valid[:, None], chosen, jnp.zeros_like(chosen))


def mixer(queries_a, queries_b, keys_a, keys_b, values, lambdas, head_gain, w_out):
    tokens = queries_a.shape[0]
    local_heads = lambdas.shape[0]
    kv_local = keys_a.shape[1] // HEAD
    group = local_heads // kv_local
    scale = HEAD ** (-0.5)
    query_pos = lax.axis_index("ep") * tokens + jnp.arange(tokens, dtype=jnp.int32)
    grouped_a = queries_a.reshape(tokens, kv_local, group, HEAD)
    grouped_b = queries_b.reshape(tokens, kv_local, group, HEAD)
    lowest = jnp.full((kv_local, group, tokens), negative, jnp.float32)
    nothing = jnp.zeros((kv_local, group, tokens), jnp.float32)
    blank = jnp.zeros((kv_local, group, tokens, VDIM), jnp.float32)

    def one_map(grouped, keys, value_rows, visible, state):
        peak, total, accum = state
        scores = (
            jnp.einsum("rgjd,ngd->gjrn", grouped, keys, preferred_element_type=jnp.float32) * scale
        )
        scores = jnp.where(visible, scores, negative)
        new_peak = jnp.maximum(peak, jnp.max(scores, axis=-1))
        expo = jnp.where(visible, jnp.exp(scores - new_peak[..., None]), 0.0)
        total = jnp.sum(expo, axis=-1)
        accum = jnp.einsum(
            "gjrn,ngv->gjrv",
            expo.astype(jnp.bfloat16),
            value_rows,
            preferred_element_type=jnp.float32,
        )
        return (new_peak, total, accum)

    initial = (lowest, nothing, blank, lowest, nothing, blank)
    piece_a = lax.all_gather(keys_a, "ep", axis=0, tiled=True)
    piece_b = lax.all_gather(keys_b, "ep", axis=0, tiled=True)
    piece_v = lax.all_gather(values, "ep", axis=0, tiled=True)
    count = piece_a.shape[0]

    def visit(state):
        key_pos = jnp.arange(count, dtype=jnp.int32)
        visible = key_pos[None, :] <= query_pos[:, None]
        value_rows = piece_v.reshape(count, kv_local, VDIM)
        first = one_map(
            grouped_a, piece_a.reshape(count, kv_local, HEAD), value_rows, visible, state[:3]
        )
        second = one_map(
            grouped_b, piece_b.reshape(count, kv_local, HEAD), value_rows, visible, state[3:]
        )
        return first + second

    result = lax.cond(jnp.int32(0) <= query_pos[tokens - 1], visit, lambda state: state, initial)
    mixed_a = result[2] / result[1][..., None]
    mixed_b = result[5] / result[4][..., None]
    diff = mixed_a - lambdas.reshape(kv_local, group, 1, 1) * mixed_b
    heads_out = (
        diff * lax.rsqrt(jnp.mean(diff * diff, axis=-1, keepdims=True) + eps) * head_gain
    ).astype(jnp.bfloat16)
    weights_out = w_out.reshape(kv_local, group, VDIM, w_out.shape[1])
    return lax.psum_scatter(
        jnp.einsum(
            "gjrv,gjvd->rd", heads_out, weights_out, preferred_element_type=jnp.float32
        ).astype(jnp.bfloat16),
        "tp",
        scatter_dimension=0,
        tiled=True,
    )


def experts(moe_tokens, moe_gain, routes, route_weights, w_gate, w_up, w_down):
    tok_rows, width = moe_tokens.shape
    n_experts = lax.axis_size("ep") * w_gate.shape[0]
    capacity = max(2, 3 * tok_rows * TOP // (2 * n_experts))
    inputs = moe_tokens.astype(jnp.float32)
    normed = (
        inputs * lax.rsqrt(jnp.mean(inputs * inputs, axis=-1, keepdims=True) + eps) * moe_gain
    ).astype(jnp.bfloat16)
    chosen = routes.reshape(-1)
    member = (chosen[:, None] == jnp.arange(n_experts, dtype=jnp.int32)[None, :]).astype(jnp.int32)
    order_in = jnp.sum(jnp.cumsum(member, axis=0) * member, axis=1) - 1
    slot_ids = chosen * capacity + order_in
    owner = (
        jnp.full((n_experts * capacity,), tok_rows, jnp.int32)
        .at[slot_ids]
        .set(jnp.arange(tok_rows * TOP, dtype=jnp.int32) // TOP)
    )
    outgoing = pick_rows(normed, owner).reshape(n_experts, capacity, width)
    arrived = lax.all_to_all(outgoing, "ep", split_axis=0, concat_axis=1, tiled=True).reshape(
        -1, width
    )
    hidden = hidden_rows(lax.all_gather(arrived, "tp", axis=0, tiled=True), w_gate[0], w_up[0])
    expert_out = lax.psum_scatter(
        jnp.dot(hidden, w_down[0], preferred_element_type=jnp.float32).astype(jnp.bfloat16),
        "tp",
        scatter_dimension=0,
        tiled=True,
    )
    returned = lax.all_to_all(
        expert_out.reshape(-1, capacity, width), "ep", split_axis=0, concat_axis=0, tiled=True
    )
    picked = jnp.take(returned.reshape(-1, width), slot_ids, axis=0).reshape(tok_rows, TOP, width)
    return jnp.sum(picked.astype(jnp.float32) * route_weights[:, :, None], axis=1).astype(
        jnp.bfloat16
    )


def body(
    queries_a,
    queries_b,
    keys_a,
    keys_b,
    values,
    lambdas,
    head_gain,
    w_out,
    moe_tokens,
    moe_gain,
    routes,
    route_weights,
    w_gate,
    w_up,
    w_down,
):
    mixer_out = mixer(queries_a, queries_b, keys_a, keys_b, values, lambdas, head_gain, w_out)
    moe_out = experts(moe_tokens, moe_gain, routes, route_weights, w_gate, w_up, w_down)
    return (mixer_out, moe_out)


def solution(mesh):
    return jax.shard_map(
        body,
        mesh=mesh,
        in_specs=(
            P("ep", "tp"),
            P("ep", "tp"),
            P("ep", "tp"),
            P("ep", "tp"),
            P("ep", "tp"),
            P("tp"),
            P(),
            P("tp", None),
            P(("ep", "tp"), None),
            P(),
            P(("ep", "tp"), None),
            P(("ep", "tp"), None),
            P("ep", None, "tp"),
            P("ep", None, "tp"),
            P("ep", "tp", None),
        ),
        out_specs=(P(("ep", "tp"), None), P(("ep", "tp"), None)),
        check_vma=False,
    )
```

profile of v0, /device:TPU:0, one launch (start us, length us, event | category | flops | bytes accessed | tf_op | source)
XLA Modules:
  0.0 350.4 jit_solution(3916929698931288925)
XLA Ops:
  10.3 1.4 scatter_custom_fusion
  12.0 1.2 fusion.27
  13.2 1.2 fusion.29
  14.5 3.1 gather_fusion
  17.6 1.7 select_select_fusion
  19.3 44.2 %all_to_all.14 = bf16[8,48,2048]{2,1,0:T(8,128)(2,1)} all-to-all(bf16[8,48,2048]{2,1,0:T(8,128)(2,1)S(1)} %select_select_fusion), channel_id=1, replica_groups=mesh['ep'=8,'tp'=4] {'ep'}, dimensions={0} | all-to-all | bytes 3145728 | tf_op jit(solution)/shard_map/all_to_all | solution.py:119
  63.5 45.5 %all-gather.2.cloned.1.call-done = bf16[1536,2048]{1,0:T(8,128)(2,1)} async-done(((bf16[384,2048]{1,0:T(8,128)(2,1)}), bf16[1536,2048]{1,0:T(8,128)(2,1)}) %all-gather.2.cloned.1.call-update) | async-done | bytes 6291472 | tf_op jit(solution)/shard_map/all_gather | solution.py:122
  109.0 8.5 %convolution_minimum_fusion = f32[1536,512]{1,0:T(8,128)} fusion(bf16[1536,2048]{1,0:T(8,128)(2,1)} %all-gather.2.cloned.1.call-done, bf16[1,2048,512]{2,1,0:T(8,128)(2,1)} %param.29), kind=kOutput, calls=%fused_computation.30 | convolution fusion | flops 3222011904 | bytes 11534336 | tf_op jit(solution)/shard_map/dot_general | solution.py:24
  117.5 11.9 %convolution_convert_fusion = bf16[1536,2048]{1,0:T(8,128)(2,1)} fusion(bf16[1,512,2048]{2,1,0:T(8,128)(2,1)S(1)} %copy-done, bf16[1536,2048]{1,0:T(8,128)(2,1)} %all-gather.2.cloned.1.call-done, f32[1536,512]{1,0:T(8,128)} %convolution_minimum_fusion, bf16[1,2048,512]{2,1,0:T(8,128)(2,1)} %param.30), kind=kOutput, calls=%fused_computation.28 | convolution fusion | flops 6452674560 | bytes 19922944 | tf_op jit(solution)/shard_map/dot_general | solution.py:124
  129.5 58.9 %reduce-scatter.5.cloned.1.call-done = bf16[384,2048]{1,0:T(8,128)(2,1)} async-done(((bf16[1536,2048]{1,0:T(8,128)(2,1)}), bf16[384,2048]{1,0:T(8,128)(2,1)}) %reduce-scatter.5.cloned.1.call-update) | async-done | bytes 1572880 | tf_op jit(solution)/shard_map/reduce_scatter | solution.py:123
  188.4 5.5 %all-to-all-start.1 = ((bf16[8,48,2048]{2,1,0:T(8,128)(2,1)}), bf16[8,48,2048]{2,1,0:T(8,128)(2,1)}, u32[]{:S(2)}, u32[]{:S(2)}) async-start(bf16[8,48,2048]{2,1,0:T(8,128)(2,1)} %bitcast.77), calls=%async_computation.3 | async-start | bytes 3145728 | tf_op jit(solution)/shard_map/all_to_all | solution.py:129
  196.2 54.2 %all_gather.12 = bf16[1024,128]{0,1:T(8,128)(2,1)S(1)} all-gather(bf16[128,128]{0,1:T(8,128)(2,1)S(1)} %copy.45), channel_id=1, replica_groups=mesh['ep'=8,'tp'=4] {'ep'}, dimensions={0}, use_global_device_ids=true | all-gather | bytes 294912 | tf_op jit(solution)/shard_map/all_gather | solution.py:66
  250.3 27.8 %all_gather.14 = bf16[1024,128]{0,1:T(8,128)(2,1)} all-gather(bf16[128,128]{0,1:T(8,128)(2,1)S(1)} %copy.46), channel_id=1, replica_groups=mesh['ep'=8,'tp'=4] {'ep'}, dimensions={0}, use_global_device_ids=true | all-gather | bytes 294912 | tf_op jit(solution)/shard_map/all_gather | solution.py:67
  278.2 31.3 %all_gather.13 = bf16[1024,256]{1,0:T(8,128)(2,1)S(1)} all-gather(bf16[128,256]{1,0:T(8,128)(2,1)S(1)} %copy-done.6), channel_id=1, replica_groups=mesh['ep'=8,'tp'=4] {'ep'}, dimensions={0}, use_global_device_ids=true | all-gather | bytes 589824 | tf_op jit(solution)/shard_map/all_gather | solution.py:68
  309.5 12.2 %conditional.1 = (f32[2,2,128]{2,1,0:T(2,128)S(1)}, f32[2,2,128,128]{3,2,1,0:T(8,128)S(1)}, f32[2,2,128]{2,1,0:T(2,128)S(1)}, f32[2,2,128,128]{3,2,1,0:T(8,128)S(1)}) conditional(s32[]{:T(128)} %bitcast.12, () %tuple.16, (s32[128]{0:T(128)S(1)}, bf16[1024,128]{0,1:T(8,128)(2,1)S(1)}, bf16[128,256]{1,0:T(8,128)(2,1)}, bf16[1024,256]{1,0:T(8,128)(2,1)S(1)}, ...), branch_computations={%region_0.0_spmd, %region_1.6_spmd} | conditional | flops 416414720 | bytes 47481572 | solution.py:83
  310.6 1.8 fusion.42
  312.5 2.4 fusion.1
  317.2 2.6 fusion.6
  319.8 1.9 fusion.8
  322.7 2.9 fusion.23
  326.2 4.0 %gather_fusion.1 = bf16[256,2048]{1,0:T(8,128)(2,1)S(1)} fusion(bf16[384,2048]{1,0:T(8,128)(2,1)} %bitcast.26, s32[1024]{0:T(1024)S(1)} %pad_clamp_fusion), kind=kCustom, calls=%fused_computation.1 | custom fusion | bytes 2098176 | tf_op jit(solution)/shard_map/jit(_take)/gather | solution.py:132
  330.2 1.5 gather.15
  331.7 6.2 %multiply_reduce_fusion = bf16[128,2048]{1,0:T(8,128)(2,1)} fusion(bf16[128,2,2048]{2,1,0:T(2,128)(2,1)} %gather.15, pred[128,2]{1,0:T(8,128)(4,1)S(1)} %copy.52, f32[128,2]{1,0:T(8,128)S(1)} %copy.54), kind=kLoop, calls=%fused_computation.39 | loop fusion | flops 1835008 | bytes 1574144 | tf_op jit(solution)/shard_map/reduce_sum | solution.py:133
  338.0 5.9 %reduce-scatter.3.cloned.1.call-done = bf16[32,2048]{1,0:T(8,128)(2,1)} async-done(((bf16[128,2048]{1,0:T(8,128)(2,1)}), bf16[32,2048]{1,0:T(8,128)(2,1)}) %reduce-scatter.3.cloned.1.call-update) | async-done | bytes 131088 | tf_op jit(solution)/shard_map/reduce_scatter | solution.py:91
  (79 shorter events, 9.8 us)
Async XLA Ops:
  7.2 110.4 %copy-start = (bf16[1,512,2048]{2,1,0:T(8,128)(2,1)S(1)}, bf16[1,512,2048]{2,1,0:T(8,128)(2,1)}, u32[]{:S(2)}) copy-start(bf16[1,512,2048]{2,1,0:T(8,128)(2,1)} %param.31) | copy-start | bytes 6291460
  7.2 101.8 %all-gather.2.cloned.1.call-start = ((), (), s32[]{:S(2)}) async-start(), calls=%async_computation.5 | async-start | bytes 7864320 | tf_op jit(solution)/shard_map/all_gather | solution.py:122
  10.3 1.4 copy-start.12
  63.5 124.9 %reduce-scatter.5.cloned.1.call-start = ((), (), s32[]{:S(2)}) async-start(), calls=%async_computation.6 | async-start | bytes 7864320 | tf_op jit(solution)/shard_map/reduce_scatter | solution.py:123
  129.4 64.6 %copy-start.8 = (bf16[128,128]{1,0:T(8,128)(2,1)S(1)}, bf16[128,128]{1,0:T(8,128)(2,1)}, u32[]{:S(2)}) copy-start(bf16[128,128]{1,0:T(8,128)(2,1)} %param.19) | copy-start | bytes 98308
  129.4 64.7 %copy-start.9 = (bf16[128,128]{1,0:T(8,128)(2,1)S(1)}, bf16[128,128]{1,0:T(8,128)(2,1)}, u32[]{:S(2)}) copy-start(bf16[128,128]{1,0:T(8,128)(2,1)} %param.20) | copy-start | bytes 98308
  129.5 66.0 %copy-start.15 = (f32[4]{0:T(128)S(1)}, f32[4]{0:T(128)}, u32[]{:S(2)}) copy-start(f32[4]{0:T(128)} %param.22) | copy-start | bytes 52
  129.5 148.7 %copy-start.6 = (bf16[128,256]{1,0:T(8,128)(2,1)S(1)}, bf16[128,256]{1,0:T(8,128)(2,1)}, u32[]{:S(2)}) copy-start(bf16[128,256]{1,0:T(8,128)(2,1)} %param.21) | copy-start | bytes 196612
  188.4 137.8 %all-to-all-start.1 = ((bf16[8,48,2048]{2,1,0:T(8,128)(2,1)}), bf16[8,48,2048]{2,1,0:T(8,128)(2,1)}, u32[]{:S(2)}, u32[]{:S(2)}) async-start(bf16[8,48,2048]{2,1,0:T(8,128)(2,1)} %bitcast.77), calls=%async_computation.3 | async-start | bytes 3145728 | tf_op jit(solution)/shard_map/all_to_all | solution.py:129
  193.9 149.9 %reduce-scatter.3.cloned.1.call-start = ((), (), s32[]{:S(2)}) async-start(), calls=%async_computation.4 | async-start | bytes 655360 | tf_op jit(solution)/shard_map/reduce_scatter | solution.py:91
  309.5 2.9 copy-start.7
  309.5 3.0 copy-start.4
  312.5 2.5 copy-start.1
  315.0 1.3 copy-start.3
  315.0 1.3 copy-start.11
  316.4 0.8 copy-start.5
  317.2 2.6 copy-start.2
  321.7 4.2 %copy-start.10 = (s32[128,2]{0,1:T(2,128)S(1)}, s32[128,2]{0,1:T(2,128)}, u32[]{:S(2)}) copy-start(s32[128,2]{0,1:T(2,128)} %param.27) | copy-start | bytes 3076
  321.7 4.4 %copy-start.14 = (f32[128,2]{0,1:T(2,128)S(1)}, f32[128,2]{0,1:T(2,128)}, u32[]{:S(2)}) copy-start(f32[128,2]{0,1:T(2,128)} %param.28) | copy-start | bytes 3076
  321.7 4.5 %copy-start.13 = (s32[256,1]{0,1:T(1,128)S(1)}, s32[256,1]{0,1:T(1,128)}, u32[]{:S(2)}) copy-start(s32[256,1]{0,1:T(1,128)} %copy-done.12) | copy-start | bytes 3076
Sparse Core Ops, SparseCore 0:
  63.6 45.3 all-gather.1
  129.6 58.8 reduce-scatter.4
  325.8 18.0 reduce-scatter.2
where the time goes:
time: 351 us; the launch traced here: 350 us
  blocking collectives  158 us (45%)
  waiting for transfers between devices  110 us (31%)
  matrix products  32.1 us (9%)
  local copies, waits for them, and re-layouts  16.1 us (5%)
  between operations  14.7 us (4%)
  other arithmetic  14 us (4%)
  starting transfers between devices  5.63 us (2%)
    reduce_scatter x1, waiting for transfers between devices, experts(): lax.psum_scatter(jnp.dot(hidden, w_down[0], preferred_element_type=jnp.fl...  58.9 us
    all_gather x1, blocking collectives, mixer(): piece_a = lax.all_gather(keys_a, 'ep', axis=0, tiled=True)  54.2 us
    all_gather x1, waiting for transfers between devices, experts(): lax.all_gather(arrived, 'tp', axis=0, tiled=True)  45.5 us
    all_to_all x1, blocking collectives, experts(): lax.all_to_all(outgoing, 'ep', split_axis=0, concat_axis=1, tiled=True)  44.2 us
    all_gather x1, blocking collectives, mixer(): piece_v = lax.all_gather(values, 'ep', axis=0, tiled=True)  31.3 us
    all_gather x1, blocking collectives, mixer(): piece_b = lax.all_gather(keys_b, 'ep', axis=0, tiled=True)  27.8 us
    dot_general x1, matrix products, experts(): jnp.dot(hidden, w_down[0], preferred_element_type=jnp.float32)  11.9 us
    dot_general x1, matrix products, hidden_rows(): gate = jnp.dot(inputs, gate_matrix, preferred_element_type=jnp.float32)  8.52 us
  transfers between devices with their start and end apart: 4, of which 3 were waited for; matrix products, arithmetic and copies ran while one was open for 8% of the time, Pallas kernels for 0%

commit v1 on v0

--- a/solution.py
+++ b/solution.py
@@ -1,6 +1,10 @@
+import functools
+
 import jax
 import jax.numpy as jnp
 from jax import lax
+from jax.experimental import pallas as pl
+from jax.experimental.pallas import tpu as pltpu
 from jax.sharding import PartitionSpec as P
 
 HEAD = 64
@@ -157,9 +161,387 @@
     return (mixer_out, moe_out)
 
 
+MESH = pl.DeviceIdType.MESH
+OUT, CORE, ACROSS, CORE_ACROSS, PART, PAIR, SUMS, BACK, KV_Z, KV_Y = range(10)
+
+
+def xor(first, second, limit):
+    total, bit = 0, 1
+    while bit < limit:
+        total = total + (first // bit + second // bit) % 2 * bit
+        bit *= 2
+    return total
+
+
+def exchange(
+    n, outgoing, kv, w_gate, w_up, w_down, ret, kv_all,
+    rows, parts, part_in, pair_in, sums_in, sums, final, hidden, gate_v, up_v, down_v,
+    send, recv, local,
+):
+    me = lax.axis_index("ep")
+    tp = lax.axis_index("tp")
+    core = tp + 1 - 2 * (tp % 2)
+    across = tp + 2 - 4 * (tp // 2)
+    cap, width = outgoing.shape[1:]
+    units = hidden.shape[1]
+    flat = 4 * cap
+
+    def mask_of(k):
+        return 2 * ((n // 2 - k // 2) % (n // 2)) + k % 2
+
+    def partner(k):
+        return xor(me, mask_of(k), n)
+
+    def copy(kind, k, source, target, device):
+        return pltpu.make_async_remote_copy(
+            src_ref=source,
+            dst_ref=target,
+            send_sem=send.at[kind, k],
+            recv_sem=recv.at[kind, k],
+            device_id=device,
+            device_id_type=MESH,
+        )
+
+    def out_copy(k):
+        return copy(OUT, k, outgoing.at[partner(k)], rows.at[k, 0], {"ep": partner(k)})
+
+    def core_copy(k):
+        return copy(CORE, k, rows.at[k, 0], rows.at[k, 1], {"tp": core})
+
+    def across_copy(k):
+        return copy(ACROSS, k, rows.at[k, 0], rows.at[k, 2], {"tp": across})
+
+    def core_across_copy(k):
+        return copy(CORE_ACROSS, k, rows.at[k, 2], rows.at[k, 3], {"tp": core})
+
+    def part_copy(k):
+        return copy(PART, k, parts.at[k, 1], part_in.at[k], {"tp": core})
+
+    def pair_copy(k):
+        return copy(PAIR, k, parts.at[k, 3], pair_in.at[k], {"tp": core})
+
+    def sums_copy(k):
+        return copy(SUMS, k, sums.at[k], sums_in.at[k], {"tp": across})
+
+    def back_copy(k):
+        return copy(BACK, k, final.at[k], ret.at[me], {"ep": partner(k)})
+
+    def kv_z_copy(z):
+        return copy(KV_Z, z, kv, kv_all.at[me], {"ep": xor(me, 2 * z, n)})
+
+    def kv_y_copy(z):
+        source = xor(me, 2 * z, n)
+        return copy(KV_Y, z, kv_all.at[source], kv_all.at[source], {"ep": xor(me, 1, n)})
+
+    own = pltpu.make_async_copy(outgoing.at[me], rows.at[0, 0], local.at[0])
+    own.start()
+    own_kv = pltpu.make_async_copy(kv, kv_all.at[me], local.at[1])
+    own_kv.start()
+    loads = [
+        pltpu.make_async_copy(w_gate, gate_v, local.at[2]),
+        pltpu.make_async_copy(w_up, up_v, local.at[3]),
+        pltpu.make_async_copy(w_down, down_v, local.at[4]),
+    ]
+    for load in loads:
+        load.start()
+
+    barrier = pltpu.get_barrier_semaphore()
+    for shift in range(1, n):
+        pl.semaphore_signal(
+            barrier, inc=1, device_id={"ep": (me + shift) % n}, device_id_type=MESH
+        )
+    for shift in range(1, 4):
+        pl.semaphore_signal(
+            barrier, inc=1, device_id={"tp": (tp + shift) % 4}, device_id_type=MESH
+        )
+    pl.semaphore_wait(barrier, n + 2)
+
+    own.wait()
+    core_copy(0).start()
+    across_copy(0).start()
+
+    @pl.loop(1, n)
+    def _(k):
+        out_copy(k).start()
+
+    for z in range(1, n // 2):
+        kv_z_copy(z).start()
+    own_kv.wait()
+    for load in loads:
+        load.wait()
+
+    @pl.loop(0, n + 2)
+    def _(k):
+        @pl.when(k + 1 < n)
+        def _():
+            out_copy(k + 1).wait_recv()
+            core_copy(k + 1).start()
+            across_copy(k + 1).start()
+
+        @pl.when(k < n)
+        def _():
+            across_copy(k).wait_recv()
+            core_across_copy(k).start()
+            core_copy(k).wait_recv()
+            core_across_copy(k).wait_recv()
+            inputs = rows[k].reshape(flat, width)
+            step = min(256, units)
+            for first in range(0, units, step):
+                gate = jnp.dot(
+                    inputs, gate_v[:, first : first + step], preferred_element_type=jnp.float32
+                )
+                up = jnp.dot(
+                    inputs, up_v[:, first : first + step], preferred_element_type=jnp.float32
+                )
+                hidden[:, first : first + step] = clamped_unit(gate, up).astype(jnp.bfloat16)
+            for first in range(0, width, 256):
+                piece = jnp.dot(
+                    hidden[...], down_v[:, first : first + 256], preferred_element_type=jnp.float32
+                )
+                parts[k, :, :, first : first + 256] = piece.astype(jnp.bfloat16).reshape(
+                    4, cap, 256
+                )
+            pair_copy(k).start()
+            part_copy(k).start()
+
+        @pl.when((k >= 1) & (k <= n))
+        def _():
+            j = k - 1
+            pair_copy(j).wait_recv()
+            sums[j] = (
+                parts[j, 2].astype(jnp.float32) + pair_in[j].astype(jnp.float32)
+            ).astype(jnp.bfloat16)
+            sums_copy(j).start()
+
+        @pl.when(k >= 2)
+        def _():
+            j = k - 2
+            part_copy(j).wait_recv()
+            sums_copy(j).wait_recv()
+            final[j] = (
+                parts[j, 0].astype(jnp.float32)
+                + part_in[j].astype(jnp.float32)
+                + sums_in[j].astype(jnp.float32)
+            ).astype(jnp.bfloat16)
+
+            @pl.when(j >= 1)
+            def _():
+                back_copy(j).start()
+
+        @pl.when(k == n // 2)
+        def _():
+            for z in range(n // 2):
+                if z:
+                    kv_z_copy(z).wait_recv()
+                kv_y_copy(z).start()
+
+    ret[me] = final[0]
+    for z in range(n // 2):
+        if z:
+            kv_z_copy(z).wait_send()
+        kv_y_copy(z).wait_send()
+        kv_y_copy(z).wait_recv()
+
+    @pl.loop(0, n)
+    def _(k):
+        for made in (core_copy, across_copy, core_across_copy, part_copy, pair_copy, sums_copy):
+            made(k).wait_send()
+
+        @pl.when(k >= 1)
+        def _():
+            out_copy(k).wait_send()
+            back_copy(k).wait_send()
+            back_copy(k).wait_recv()
+
+
+def run_exchange(n, outgoing, kv, w_gate, w_up, w_down):
+    _, cap, width = outgoing.shape
+    units = w_gate.shape[1]
+    block = (n, cap, width)
+    vmem = pl.BlockSpec(memory_space=pltpu.VMEM)
+    hbm = pl.BlockSpec(memory_space=pl.ANY)
+    return pl.pallas_call(
+        functools.partial(exchange, n),
+        out_shape=(
+            jax.ShapeDtypeStruct(block, jnp.bfloat16),
+            jax.ShapeDtypeStruct((n,) + kv.shape, jnp.bfloat16),
+        ),
+        in_specs=[vmem, vmem, hbm, hbm, hbm],
+        out_specs=(vmem, vmem),
+        scratch_shapes=[
+            pltpu.VMEM((n, 4, cap, width), jnp.bfloat16),
+            pltpu.VMEM((n, 4, cap, width), jnp.bfloat16),
+            pltpu.VMEM(block, jnp.bfloat16),
+            pltpu.VMEM(block, jnp.bfloat16),
+            pltpu.VMEM(block, jnp.bfloat16),
+            pltpu.VMEM(block, jnp.bfloat16),
+            pltpu.VMEM(block, jnp.bfloat16),
+            pltpu.VMEM((4 * cap, units), jnp.bfloat16),
+            pltpu.VMEM(w_gate.shape, jnp.bfloat16),
+            pltpu.VMEM(w_up.shape, jnp.bfloat16),
+            pltpu.VMEM(w_down.shape, jnp.bfloat16),
+            pltpu.SemaphoreType.DMA((10, n)),
+            pltpu.SemaphoreType.DMA((10, n)),
+            pltpu.SemaphoreType.DMA((5,)),
+        ],
+        compiler_params=pltpu.CompilerParams(
+            collective_id=0, has_side_effects=True, vmem_limit_bytes=60 * 2**20
+        ),
+        name="exchange",
+    )(outgoing, kv, w_gate, w_up, w_down)
+
+
+def scatter_sum(n, parts, out, landed, send, recv):
+    me = lax.axis_index("tp")
+    barrier = pltpu.get_barrier_semaphore()
+    for shift in range(1, n):
+        pl.semaphore_signal(
+            barrier, inc=1, device_id={"tp": (me + shift) % n}, device_id_type=MESH
+        )
+    pl.semaphore_wait(barrier, n - 1)
+    copies = []
+    for shift in range(1, n):
+        target = (me + shift) % n
+        copies.append(
+            pltpu.make_async_remote_copy(
+                src_ref=parts.at[target],
+                dst_ref=landed.at[shift - 1],
+                send_sem=send.at[shift - 1],
+                recv_sem=recv.at[shift - 1],
+                device_id={"tp": target},
+                device_id_type=MESH,
+            )
+        )
+        copies[-1].start()
+    total = parts[me].astype(jnp.float32)
+    for shift in range(1, n):
+        copies[shift - 1].wait_recv()
+        total = total + landed[shift - 1].astype(jnp.float32)
+    out[...] = total.astype(jnp.bfloat16)
+    for made in copies:
+        made.wait_send()
+
+
+def run_scatter_sum(n, parts):
+    count, width = parts.shape[0] // n, parts.shape[1]
+    vmem = pl.BlockSpec(memory_space=pltpu.VMEM)
+    return pl.pallas_call(
+        functools.partial(scatter_sum, n),
+        out_shape=jax.ShapeDtypeStruct((count, width), jnp.bfloat16),
+        in_specs=[vmem],
+        out_specs=vmem,
+        scratch_shapes=[
+            pltpu.VMEM((n - 1, count, width), jnp.bfloat16),
+            pltpu.SemaphoreType.DMA((n - 1,)),
+            pltpu.SemaphoreType.DMA((n - 1,)),
+        ],
+        compiler_params=pltpu.CompilerParams(collective_id=1, has_side_effects=True),
+        name="scatter_sum",
+    )(parts.reshape(n, count, width))
+
+
+def attend(queries_a, queries_b, kv_all, lambdas, head_gain, w_out, n_tp):
+    tokens = queries_a.shape[0]
+    local_heads = lambdas.shape[0]
+    kv_rows = kv_all.reshape(-1, kv_all.shape[-1])
+    count = kv_rows.shape[0]
+    kv_local = kv_rows.shape[1] // (2 * HEAD + VDIM)
+    group = local_heads // kv_local
+    scale = HEAD ** (-0.5)
+    span = kv_local * HEAD
+    query_pos = lax.axis_index("ep") * tokens + jnp.arange(tokens, dtype=jnp.int32)
+    key_pos = jnp.arange(count, dtype=jnp.int32)
+    visible = key_pos[None, :] <= query_pos[:, None]
+    value_rows = kv_rows[:, 2 * span :].reshape(count, kv_local, VDIM)
+
+    def one_map(queries, keys):
+        grouped = queries.reshape(tokens, kv_local, group, HEAD)
+        scores = (
+            jnp.einsum(
+                "rgjd,ngd->gjrn",
+                grouped,
+                keys.reshape(count, kv_local, HEAD),
+                preferred_element_type=jnp.float32,
+            )
+            * scale
+        )
+        scores = jnp.where(visible, scores, negative)
+        peak = jnp.max(scores, axis=-1, keepdims=True)
+        expo = jnp.where(visible, jnp.exp(scores - peak), 0.0)
+        total = jnp.sum(expo, axis=-1, keepdims=True)
+        mixed = jnp.einsum(
+            "gjrn,ngv->gjrv",
+            expo.astype(jnp.bfloat16),
+            value_rows,
+            preferred_element_type=jnp.float32,
+        )
+        return mixed / total
+
+    first = one_map(queries_a, kv_rows[:, :span])
+    second = one_map(queries_b, kv_rows[:, span : 2 * span])
+    diff = first - lambdas.reshape(kv_local, group, 1, 1) * second
+    heads_out = (
+        diff * lax.rsqrt(jnp.mean(diff * diff, axis=-1, keepdims=True) + eps) * head_gain
+    ).astype(jnp.bfloat16)
+    weights_out = w_out.reshape(kv_local, group, VDIM, w_out.shape[1])
+    parts = jnp.einsum(
+        "gjrv,gjvd->rd", heads_out, weights_out, preferred_element_type=jnp.float32
+    ).astype(jnp.bfloat16)
+    return run_scatter_sum(n_tp, parts)
+
+
+def fast_body(
+    queries_a, queries_b, keys_a, keys_b, values, lambdas, head_gain, w_out,
+    moe_tokens, moe_gain, routes, route_weights, w_gate, w_up, w_down,
+):
+    n, n_tp = lax.axis_size("ep"), lax.axis_size("tp")
+    tok_rows, width = moe_tokens.shape
+    cap = 3 * tok_rows * TOP // (2 * n)
+    inputs = moe_tokens.astype(jnp.float32)
+    normed = (
+        inputs * lax.rsqrt(jnp.mean(inputs * inputs, axis=-1, keepdims=True) + eps) * moe_gain
+    ).astype(jnp.bfloat16)
+    named = routes[:, :, None] == jnp.arange(n, dtype=jnp.int32)[None, None, :]
+    member = jnp.any(named, axis=1)
+    earlier = jnp.tril(jnp.ones((tok_rows, tok_rows), jnp.bfloat16), -1)
+    place = jnp.dot(
+        earlier, member.astype(jnp.bfloat16), preferred_element_type=jnp.float32
+    ).astype(jnp.int32)
+    slot = jnp.where(member, place, cap).T
+    pick = (slot[:, None, :] == jnp.arange(cap, dtype=jnp.int32)[None, :, None]).reshape(
+        n * cap, tok_rows
+    )
+    outgoing = (
+        jnp.dot(pick.astype(jnp.bfloat16), normed, preferred_element_type=jnp.float32)
+        .astype(jnp.bfloat16)
+        .reshape(n, cap, width)
+    )
+    kv = jnp.concatenate([keys_a, keys_b, values], axis=1)
+    returned, kv_all = run_exchange(n, outgoing, kv, w_gate[0], w_up[0], w_down[0])
+    mixer_out = attend(queries_a, queries_b, kv_all, lambdas, head_gain, w_out, n_tp)
+    slot_ids = routes * cap + jnp.sum(jnp.where(named, place[:, None, :], 0), axis=2)
+    table = returned.reshape(n * cap, width)
+    total = 0.0
+    for k in range(TOP):
+        chosen = slot_ids[:, k : k + 1] == jnp.arange(n * cap, dtype=jnp.int32)[None, :]
+        total = total + route_weights[:, k : k + 1] * jnp.dot(
+            chosen.astype(jnp.bfloat16), table, preferred_element_type=jnp.float32
+        )
+    return (mixer_out, total.astype(jnp.bfloat16))
+
+
+def whole_body(*args):
+    n, n_tp = lax.axis_size("ep"), lax.axis_size("tp")
+    tok_rows, w_gate = args[8].shape[0], args[12]
+    cap = 3 * tok_rows * TOP // (2 * n)
+    if w_gate.shape[0] == 1 and n_tp == 4 and n & (n - 1) == 0 and n >= 4 and cap % 16 == 0:
+        return fast_body(*args)
+    return body(*args)
+
+
 def solution(mesh):
     return jax.shard_map(
-        body,
+        whole_body,
         mesh=mesh,
         in_specs=(
             P("ep", "tp"),

time: 351 us -> 154 us (0.44)
  blocking collectives: 158 us -> 0 us
  Pallas kernels: 0 us -> 112 us
  waiting for transfers between devices: 110 us -> 0 us
  between operations: 14.7 us -> 0.79 us
  matrix products: 32.1 us -> 22.7 us
  other arithmetic: 14 us -> 5.74 us
  starting transfers between devices: 5.63 us -> 0 us
  local copies, waits for them, and re-layouts: 16.1 us -> 10.7 us
    all_gather x3 -> x0, blocking collectives: 113 us -> none  [the longest x1 54.2 us: mixer(): piece_a = lax.all_gather(keys_a, 'ep', axis=0, tiled=True)]
    pallas_call x0 -> x2, Pallas kernels: none -> 112 us  [the longest x1 103 us: run_exchange(): pl.pallas_call(functools.partial(exchange, n), out_shape=(jax.ShapeDtypeS...]
    reduce_scatter x2 -> x0, waiting for transfers between devices: 64.9 us -> none  [the longest x1 58.9 us: experts(): lax.psum_scatter(jnp.dot(hidden, w_down[0], preferred_element_type=jnp.fl...]
    all_gather x1 -> x0, waiting for transfers between devices: 45.5 us -> none  [experts(): lax.all_gather(arrived, 'tp', axis=0, tiled=True)]
    all_to_all x1 -> x0, blocking collectives: 44.2 us -> none  [experts(): lax.all_to_all(outgoing, 'ep', split_axis=0, concat_axis=1, tiled=True)]
    dot_general x5 -> x7, matrix products: 27.6 us -> 11.3 us  [the longest x2 3.67 us: one_map(): jnp.einsum('rgjd,ngd->gjrn', grouped, keys.reshape(count, kv_local, HEAD)...]
    gather x3 -> x0, local copies, waits for them, and re-layouts: 8.64 us -> none  [the longest x2 5.5 us: experts(): jnp.take(returned.reshape(-1, width), slot_ids, axis=0)]
    reduce_sum x5 -> x2, other arithmetic: 9.56 us -> 1.94 us  [the longest x1 1.23 us: fast_body(): jnp.mean(inputs * inputs, axis=-1, keepdims=True) + eps]
  transfers between devices with their start and end apart: 4 -> 0, of which waited for: 3 -> 0; matrix products, arithmetic and copies ran while one was open for 8% -> 0% of each run, Pallas kernels for 0% -> 0%
where the time goes in v1:
time: 154 us; the launch traced here: 152 us
  Pallas kernels  112 us (73%)
  matrix products  22.7 us (15%)
  local copies, waits for them, and re-layouts  10.7 us (7%)
  other arithmetic  5.74 us (4%)
    pallas_call x1, Pallas kernels, run_exchange(): pl.pallas_call(functools.partial(exchange, n), out_shape=(jax.ShapeDtypeS...  103 us
    pallas_call x1, Pallas kernels, run_scatter_sum(): pl.pallas_call(functools.partial(scatter_sum, n), out_shape=jax.ShapeDtyp...  8.98 us
    dot_general x2, matrix products, one_map(): jnp.einsum('gjrn,ngv->gjrv', expo.astype(jnp.bfloat16), value_rows, prefe...  8.25 us
    unnamed x15, local copies, waits for them, and re-layouts  5.07 us
    dot_general x2, matrix products, one_map(): jnp.einsum('rgjd,ngd->gjrn', grouped, keys.reshape(count, kv_local, HEAD)...  3.67 us
    dot_general x2, matrix products, fast_body(): jnp.dot(chosen.astype(jnp.bfloat16), table, preferred_element_type=jnp.fl...  3.3 us
    sub x2, matrix products, one_map(): expo = jnp.where(visible, jnp.exp(scores - peak), 0.0)  3.12 us

profile of v1, /device:TPU:0, one launch (start us, length us, event | category | flops | bytes accessed | tf_op | source)
XLA Modules:
  0.0 152.3 jit_solution(3433700225970457392)
XLA Ops:
  0.7 1.6 %copy-done = bf16[512,2048]{1,0:T(8,128)(2,1)S(1)} copy-done((bf16[512,2048]{1,0:T(8,128)(2,1)S(1)}, bf16[512,2048]{1,0:T(8,128)(2,1)}, u32[]{:S(2)}) %copy-start) | copy-done | bytes 2097176
  2.2 1.2 fusion.9
  4.2 1.3 mul.97
  5.5 0.8 slice_bitcast_fusion.1
  8.0 1.0 copy.38
  9.0 1.0 copy.42
  10.0 0.7 iota_compare_fusion
  10.7 1.5 %pad_maximum_fusion.kv = bf16[128,512]{1,0:T(8,128)(2,1)} fusion(bf16[128,256]{1,0:T(8,128)(2,1)} %param.19, bf16[128,128]{1,0:T(8,128)(2,1)} %param.18, bf16[128,128]{1,0:T(8,128)(2,1)} %param.17), kind=kLoop, calls=%fused_computation.43 | loop fusion | flops 393216 | bytes 262144 | tf_op jit(solution)/shard_map/concatenate | solution.py:519
  12.2 2.8 %convolution_convert_fusion = bf16[384,2048]{1,0:T(8,128)(2,1)} fusion(pred[384,128]{1,0:T(32,128)(4,1)S(1)} %bitcast_compare_fusion, bf16[128,2048]{1,0:T(8,128)(2,1)} %param.23, f32[2048]{0:T(1024)} %param.24, f32[128]{0:T(128)S(1)} %add_rsqrt_fusion.1), kind=kOutput, calls=%fused_computation.2 | convolution fusion | flops 203161600 | bytes 2155008 | tf_op jit(solution)/shard_map/dot_general | solution.py:515
  15.1 103.4 %exchange.1 = (bf16[8,48,2048]{2,1,0:T(8,128)(2,1)}, bf16[8,128,512]{2,1,0:T(8,128)(2,1)}) custom-call(bf16[8,48,2048]{2,1,0:T(8,128)(2,1)} %bitcast.85, bf16[128,512]{1,0:T(8,128)(2,1)} %pad_maximum_fusion.kv, bf16[2048,512]{1,0:T(8,128)(2,1)} %bitcast.87, bf16[2048,512]{1,0:T(8,128)(2,1)} %bitcast.88, bf16[512,2048]{1,0:T(8,128)(2,1)} %bitcast.89), custom_call_target="tpu_custom_call" | custom-call | tf_op jit(solution)/shard_map/exchange/pallas_call | solution.py:363
  118.4 1.1 slice.28
  119.5 1.1 fusion.55
  120.8 1.0 copy.39
  121.8 2.1 %fusion.57 = f32[2,2,128]{2,1,0:T(2,128)S(1)} fusion(pred[128,1024]{0,1:T(8,128)(4,1)} %iota_compare_fusion, bf16[1024,2,64,1]{0,2,3,1:T(8,128)(2,1)S(1)} %bitcast.90, bf16[128,2,2,64]{0,3,2,1:T(8,128)(2,1)S(1)} %bitcast.98), kind=kOutput, calls=%fused_computation.82 | convolution fusion | flops 69731328 | bytes 460800 | tf_op jit(solution)/shard_map/sub | solution.py:470
  124.0 1.0 fusion.56
  125.1 2.0 %convolution_multiply_fusion.1 = f32[128,2048]{1,0:T(8,128)S(1)} fusion(bf16[384,2048]{1,0:T(8,128)(2,1)} %bitcast.83, f32[128]{0:T(128)S(1)} %get-tuple-element.11, s32[128]{0:T(128)S(1)} %get-tuple-element.9), kind=kOutput, calls=%fused_computation.5 | convolution fusion | flops 201637888 | bytes 2622464 | tf_op jit(solution)/shard_map/dot_general | solution.py:527
  127.1 1.3 fusion.3
  128.4 1.8 %fusion.59 = f32[2,1024,128,2]{2,1,3,0:T(8,128)} fusion(bf16[1024,2,64,1]{0,2,3,1:T(8,128)(2,1)S(1)} %bitcast.93, bf16[128,2,2,64]{0,3,2,1:T(8,128)(2,1)S(1)} %bitcast.101), kind=kOutput, calls=%fused_computation.84 | convolution fusion | flops 67108864 | bytes 2424832 | tf_op jit(solution)/shard_map/rgjd,ngd->gjrn/dot_general | solution.py:460
  130.2 4.4 %fusion.7 = f32[2,2,128,128]{2,3,1,0:T(8,128)} fusion(bf16[1024,2,128,1]{0,2,3,1:T(8,128)(2,1)S(1)} %bitcast.96, f32[2,1024,128,2]{2,1,3,0:T(8,128)} %fusion.59, pred[128,1024]{0,1:T(8,128)(4,1)S(1)} %copy-done.3, f32[2,2,128]{2,1,0:T(2,128)S(1)} %fusion.56, f32[2,2]{1,0:T(2,128)S(1)} %copy-done.5), kind=kOutput, calls=%fused_computation.18 | convolution fusion | flops 136971776 | bytes 3016720 | tf_op jit(solution)/shard_map/gjrn,ngv->gjrv/dot_general | solution.py:472
  134.7 1.8 %fusion.58 = f32[2,1024,128,2]{2,1,3,0:T(8,128)} fusion(bf16[1024,2,64,1]{0,2,3,1:T(8,128)(2,1)S(1)} %bitcast.91, bf16[128,2,2,64]{0,3,2,1:T(8,128)(2,1)S(1)} %bitcast.99), kind=kOutput, calls=%fused_computation.83 | convolution fusion | flops 67108864 | bytes 2424832 | tf_op jit(solution)/shard_map/rgjd,ngd->gjrn/dot_general | solution.py:460
  136.5 3.8 %multiply_reduce_fusion = (f32[2,2,128]{2,1,0:T(2,128)S(1)}, f32[2,2,128,128]{2,3,1,0:T(8,128)S(1)}) fusion(f32[2,2,128,128]{2,3,1,0:T(8,128)} %fusion.7, f32[2,2,128]{2,1,0:T(2,128)S(1)} %fusion.57, bf16[1024,2,128,1]{0,2,3,1:T(8,128)(2,1)S(1)} %bitcast.97, f32[2,1024,128,2]{2,1,3,0:T(8,128)} %fusion.58, pred[128,1024]{0,1:T(8,128)(4,1)S(1)} %copy-done.3), kind=kOutput, calls=%fused_computation.37 | convolution fusion | flops 137102336 | bytes 3280896 | tf_op jit(solution)/shard_map/gjrn,ngv->gjrv/dot_general | solution.py:472
  140.4 1.3 fusion.4
  141.7 9.0 %scatter_sum.1 = bf16[32,2048]{1,0:T(8,128)(2,1)} custom-call(bf16[4,32,2048]{2,1,0:T(8,128)(2,1)} %bitcast.86), custom_call_target="tpu_custom_call" | custom-call | tf_op jit(solution)/shard_map/scatter_sum/pallas_call | solution.py:428
  150.7 1.6 %copy.55 = bf16[32,2048]{1,0:T(8,128)(2,1)} copy(bf16[32,2048]{1,0:T(8,128)(2,1)} %scatter_sum.1) | data formatting | bytes 262144
  (26 shorter events, 2.8 us)
Async XLA Ops:
  0.6 1.6 %copy-start = (bf16[512,2048]{1,0:T(8,128)(2,1)S(1)}, bf16[512,2048]{1,0:T(8,128)(2,1)}, u32[]{:S(2)}) copy-start(bf16[512,2048]{1,0:T(8,128)(2,1)} %param.22) | copy-start | bytes 6291460
  121.8 2.2 %copy-start.3 = (pred[128,1024]{0,1:T(8,128)(4,1)S(1)}, pred[128,1024]{0,1:T(8,128)(4,1)}, u32[]{:S(2)}) copy-start(pred[128,1024]{0,1:T(8,128)(4,1)} %iota_compare_fusion) | copy-start | bytes 393220
  125.1 2.0 %copy-start.1 = (bf16[8,48,2048]{2,1,0:T(8,128)(2,1)S(1)}, bf16[8,48,2048]{2,1,0:T(8,128)(2,1)}, u32[]{:S(2)}) copy-start(bf16[8,48,2048]{2,1,0:T(8,128)(2,1)} %get-tuple-element.5) | copy-start | bytes 4718596
  127.1 3.2 %copy-start.2 = (bf16[1024,256]{0,1:T(8,128)(2,1)S(1)}, bf16[1024,256]{0,1:T(8,128)(2,1)}, u32[]{:S(2)}) copy-start(bf16[1024,256]{0,1:T(8,128)(2,1)} %copy.39) | copy-start | bytes 1572868
  127.1 3.1 %copy-start.5 = (f32[2,2]{1,0:T(2,128)S(1)}, f32[2,2]{1,0:T(2,128)}, u32[]{:S(2)}) copy-start(f32[2,2]{1,0:T(2,128)} %mul.97) | copy-start | bytes 52
  136.5 3.8 %copy-start.4 = (f32[128]{0:T(128)S(1)}, f32[128]{0:T(128)}, u32[]{:S(2)}) copy-start(f32[128]{0:T(128)} %param.21) | copy-start | bytes 1540

commit v2 on v1

--- a/solution.py
+++ b/solution.py
@@ -162,7 +162,7 @@
 
 
 MESH = pl.DeviceIdType.MESH
-OUT, CORE, ACROSS, CORE_ACROSS, PART, PAIR, SUMS, BACK, KV_Z, KV_Y = range(10)
+OUT, CORE, ACROSS, CORE_ACROSS, PART, PAIR, SUMS, BACK, KV_Z, KV_Y, MIX = range(11)
 
 
 def xor(first, second, limit):
@@ -174,9 +174,10 @@
 
 
 def exchange(
-    n, outgoing, kv, w_gate, w_up, w_down, ret, kv_all,
-    rows, parts, part_in, pair_in, sums_in, sums, final, hidden, gate_v, up_v, down_v,
-    send, recv, local,
+    n, outgoing, kv, queries_a, queries_b, head_gain, lambdas, w_gate, w_up, w_down, w_out,
+    ret, mixer_out,
+    rows, parts, part_in, pair_in, sums_in, sums, final, hidden, gate_v, up_v, down_v, out_v,
+    kv_all, heads, shares, landed, send, recv, local,
 ):
     me = lax.axis_index("ep")
     tp = lax.axis_index("tp")
@@ -233,6 +234,45 @@
         source = xor(me, 2 * z, n)
         return copy(KV_Y, z, kv_all.at[source], kv_all.at[source], {"ep": xor(me, 1, n)})
 
+    def mix_copy(shift):
+        target = (tp + shift) % 4
+        return copy(MIX, shift, shares.at[target], landed.at[shift - 1], {"tp": target})
+
+    tokens = kv.shape[0]
+    local_heads = heads.shape[1] // VDIM
+    kv_local = kv.shape[1] // (2 * HEAD + VDIM)
+    span = kv_local * HEAD
+
+    def one_map(queries, head, offset):
+        g = head // (local_heads // kv_local)
+        count = n * tokens
+        first = offset + g * HEAD
+        keys = kv_all[:, :, first : first + HEAD].reshape(count, HEAD)
+        first = 2 * span + g * VDIM
+        value_rows = kv_all[:, :, first : first + VDIM].reshape(count, VDIM)
+        scores = lax.dot_general(
+            queries[:, head * HEAD : (head + 1) * HEAD],
+            keys,
+            (((1,), (1,)), ((), ())),
+            preferred_element_type=jnp.float32,
+        ) * HEAD ** (-0.5)
+        query_pos = me * tokens + lax.broadcasted_iota(jnp.int32, scores.shape, 0)
+        key_pos = lax.broadcasted_iota(jnp.int32, scores.shape, 1)
+        scores = jnp.where(key_pos <= query_pos, scores, negative)
+        expo = jnp.exp(scores - jnp.max(scores, axis=1, keepdims=True))
+        total = jnp.sum(expo, axis=1, keepdims=True)
+        mixed = jnp.dot(
+            expo.astype(jnp.bfloat16), value_rows, preferred_element_type=jnp.float32
+        )
+        return mixed / total
+
+    def attend(head):
+        diff = one_map(queries_a, head, 0) - lambdas[head] * one_map(queries_b, head, span)
+        norm = lax.rsqrt(jnp.mean(diff * diff, axis=1, keepdims=True) + eps)
+        heads[:, head * VDIM : (head + 1) * VDIM] = (diff * norm * head_gain[...]).astype(
+            jnp.bfloat16
+        )
+
     own = pltpu.make_async_copy(outgoing.at[me], rows.at[0, 0], local.at[0])
     own.start()
     own_kv = pltpu.make_async_copy(kv, kv_all.at[me], local.at[1])
@@ -241,6 +281,7 @@
         pltpu.make_async_copy(w_gate, gate_v, local.at[2]),
         pltpu.make_async_copy(w_up, up_v, local.at[3]),
         pltpu.make_async_copy(w_down, down_v, local.at[4]),
+        pltpu.make_async_copy(w_out, out_v, local.at[5]),
     ]
     for load in loads:
         load.start()
@@ -260,12 +301,15 @@
     core_copy(0).start()
     across_copy(0).start()
 
-    @pl.loop(1, n)
+    for k in range(1, 4):
+        out_copy(k).start()
+    for z in range(1, n // 2):
+        kv_z_copy(z).start()
+
+    @pl.loop(4, n)
     def _(k):
         out_copy(k).start()
 
-    for z in range(1, n // 2):
-        kv_z_copy(z).start()
     own_kv.wait()
     for load in loads:
         load.wait()
@@ -282,6 +326,33 @@
         def _():
             across_copy(k).wait_recv()
             core_across_copy(k).start()
+
+        @pl.when((k >= 1) & (k <= n))
+        def _():
+            j = k - 1
+            pair_copy(j).wait_recv()
+            sums[j] = (
+                parts[j, 2].astype(jnp.float32) + pair_in[j].astype(jnp.float32)
+            ).astype(jnp.bfloat16)
+            sums_copy(j).start()
+
+        @pl.when(k >= 2)
+        def _():
+            j = k - 2
+            part_copy(j).wait_recv()
+            sums_copy(j).wait_recv()
+            final[j] = (
+                parts[j, 0].astype(jnp.float32)
+                + part_in[j].astype(jnp.float32)
+                + sums_in[j].astype(jnp.float32)
+            ).astype(jnp.bfloat16)
+
+            @pl.when(j >= 1)
+            def _():
+                back_copy(j).start()
+
+        @pl.when(k < n)
+        def _():
             core_copy(k).wait_recv()
             core_across_copy(k).wait_recv()
             inputs = rows[k].reshape(flat, width)
@@ -304,43 +375,49 @@
             pair_copy(k).start()
             part_copy(k).start()
 
-        @pl.when((k >= 1) & (k <= n))
-        def _():
-            j = k - 1
-            pair_copy(j).wait_recv()
-            sums[j] = (
-                parts[j, 2].astype(jnp.float32) + pair_in[j].astype(jnp.float32)
-            ).astype(jnp.bfloat16)
-            sums_copy(j).start()
-
-        @pl.when(k >= 2)
-        def _():
-            j = k - 2
-            part_copy(j).wait_recv()
-            sums_copy(j).wait_recv()
-            final[j] = (
-                parts[j, 0].astype(jnp.float32)
-                + part_in[j].astype(jnp.float32)
-                + sums_in[j].astype(jnp.float32)
-            ).astype(jnp.bfloat16)
-
-            @pl.when(j >= 1)
-            def _():
-                back_copy(j).start()
-
-        @pl.when(k == n // 2)
+        @pl.when(k == n // 4)
         def _():
             for z in range(n // 2):
                 if z:
                     kv_z_copy(z).wait_recv()
                 kv_y_copy(z).start()
 
+        @pl.when(k == n // 4 + 1)
+        def _():
+            for z in range(n // 2):
+                kv_y_copy(z).wait_recv()
+
+        for turn in range(4):
+
+            @pl.when(k == n // 4 + 1 + turn)
+            def _():
+                for head in range(turn, local_heads, 4):
+                    attend(head)
+
+        @pl.when(k == n // 4 + 5)
+        def _():
+            for first in range(0, width, 256):
+                piece = jnp.dot(
+                    heads[...], out_v[:, first : first + 256], preferred_element_type=jnp.float32
+                )
+                shares[:, :, first : first + 256] = piece.astype(jnp.bfloat16).reshape(
+                    4, tokens // 4, 256
+                )
+            for shift in range(1, 4):
+                mix_copy(shift).start()
+
     ret[me] = final[0]
+    total = shares[tp].astype(jnp.float32)
+    for shift in range(1, 4):
+        mix_copy(shift).wait_recv()
+        total = total + landed[shift - 1].astype(jnp.float32)
+    mixer_out[...] = total.astype(jnp.bfloat16)
+    for shift in range(1, 4):
+        mix_copy(shift).wait_send()
     for z in range(n // 2):
         if z:
             kv_z_copy(z).wait_send()
         kv_y_copy(z).wait_send()
-        kv_y_copy(z).wait_recv()
 
     @pl.loop(0, n)
     def _(k):
@@ -354,7 +431,9 @@
             back_copy(k).wait_recv()
 
 
-def run_exchange(n, outgoing, kv, w_gate, w_up, w_down):
+def run_exchange(
+    n, outgoing, kv, queries_a, queries_b, head_gain, lambdas, w_gate, w_up, w_down, w_out
+):
     _, cap, width = outgoing.shape
     units = w_gate.shape[1]
     block = (n, cap, width)
@@ -364,9 +443,9 @@
         functools.partial(exchange, n),
         out_shape=(
             jax.ShapeDtypeStruct(block, jnp.bfloat16),
-            jax.ShapeDtypeStruct((n,) + kv.shape, jnp.bfloat16),
+            jax.ShapeDtypeStruct((kv.shape[0] // 4, width), jnp.bfloat16),
         ),
-        in_specs=[vmem, vmem, hbm, hbm, hbm],
+        in_specs=[vmem] * 5 + [pl.BlockSpec(memory_space=pltpu.SMEM)] + [hbm] * 4,
         out_specs=(vmem, vmem),
         scratch_shapes=[
             pltpu.VMEM((n, 4, cap, width), jnp.bfloat16),
@@ -380,121 +459,30 @@
             pltpu.VMEM(w_gate.shape, jnp.bfloat16),
             pltpu.VMEM(w_up.shape, jnp.bfloat16),
             pltpu.VMEM(w_down.shape, jnp.bfloat16),
-            pltpu.SemaphoreType.DMA((10, n)),
-            pltpu.SemaphoreType.DMA((10, n)),
-            pltpu.SemaphoreType.DMA((5,)),
+            pltpu.VMEM(w_out.shape, jnp.bfloat16),
+            pltpu.VMEM((n,) + kv.shape, jnp.bfloat16),
+            pltpu.VMEM((kv.shape[0], w_out.shape[0]), jnp.bfloat16),
+            pltpu.VMEM((4, kv.shape[0] // 4, width), jnp.bfloat16),
+            pltpu.VMEM((3, kv.shape[0] // 4, width), jnp.bfloat16),
+            pltpu.SemaphoreType.DMA((11, n)),
+            pltpu.SemaphoreType.DMA((11, n)),
+            pltpu.SemaphoreType.DMA((6,)),
         ],
         compiler_params=pltpu.CompilerParams(
             collective_id=0, has_side_effects=True, vmem_limit_bytes=60 * 2**20
         ),
         name="exchange",
-    )(outgoing, kv, w_gate, w_up, w_down)
-
-
-def scatter_sum(n, parts, out, landed, send, recv):
-    me = lax.axis_index("tp")
-    barrier = pltpu.get_barrier_semaphore()
-    for shift in range(1, n):
-        pl.semaphore_signal(
-            barrier, inc=1, device_id={"tp": (me + shift) % n}, device_id_type=MESH
-        )
-    pl.semaphore_wait(barrier, n - 1)
-    copies = []
-    for shift in range(1, n):
-        target = (me + shift) % n
-        copies.append(
-            pltpu.make_async_remote_copy(
-                src_ref=parts.at[target],
-                dst_ref=landed.at[shift - 1],
-                send_sem=send.at[shift - 1],
-                recv_sem=recv.at[shift - 1],
-                device_id={"tp": target},
-                device_id_type=MESH,
-            )
-        )
-        copies[-1].start()
-    total = parts[me].astype(jnp.float32)
-    for shift in range(1, n):
-        copies[shift - 1].wait_recv()
-        total = total + landed[shift - 1].astype(jnp.float32)
-    out[...] = total.astype(jnp.bfloat16)
-    for made in copies:
-        made.wait_send()
-
-
-def run_scatter_sum(n, parts):
-    count, width = parts.shape[0] // n, parts.shape[1]
-    vmem = pl.BlockSpec(memory_space=pltpu.VMEM)
-    return pl.pallas_call(
-        functools.partial(scatter_sum, n),
-        out_shape=jax.ShapeDtypeStruct((count, width), jnp.bfloat16),
-        in_specs=[vmem],
-        out_specs=vmem,
-        scratch_shapes=[
-            pltpu.VMEM((n - 1, count, width), jnp.bfloat16),
-            pltpu.SemaphoreType.DMA((n - 1,)),
-            pltpu.SemaphoreType.DMA((n - 1,)),
-        ],
-        compiler_params=pltpu.CompilerParams(collective_id=1, has_side_effects=True),
-        name="scatter_sum",
-    )(parts.reshape(n, count, width))
-
-
-def attend(queries_a, queries_b, kv_all, lambdas, head_gain, w_out, n_tp):
-    tokens = queries_a.shape[0]
-    local_heads = lambdas.shape[0]
-    kv_rows = kv_all.reshape(-1, kv_all.shape[-1])
-    count = kv_rows.shape[0]
-    kv_local = kv_rows.shape[1] // (2 * HEAD + VDIM)
-    group = local_heads // kv_local
-    scale = HEAD ** (-0.5)
-    span = kv_local * HEAD
-    query_pos = lax.axis_index("ep") * tokens + jnp.arange(tokens, dtype=jnp.int32)
-    key_pos = jnp.arange(count, dtype=jnp.int32)
-    visible = key_pos[None, :] <= query_pos[:, None]
-    value_rows = kv_rows[:, 2 * span :].reshape(count, kv_local, VDIM)
-
-    def one_map(queries, keys):
-        grouped = queries.reshape(tokens, kv_local, group, HEAD)
-        scores = (
-            jnp.einsum(
-                "rgjd,ngd->gjrn",
-                grouped,
-                keys.reshape(count, kv_local, HEAD),
-                preferred_element_type=jnp.float32,
-            )
-            * scale
-        )
-        scores = jnp.where(visible, scores, negative)
-        peak = jnp.max(scores, axis=-1, keepdims=True)
-        expo = jnp.where(visible, jnp.exp(scores - peak), 0.0)
-        total = jnp.sum(expo, axis=-1, keepdims=True)
-        mixed = jnp.einsum(
-            "gjrn,ngv->gjrv",
-            expo.astype(jnp.bfloat16),
-            value_rows,
-            preferred_element_type=jnp.float32,
-        )
-        return mixed / total
-
-    first = one_map(queries_a, kv_rows[:, :span])
-    second = one_map(queries_b, kv_rows[:, span : 2 * span])
-    diff = first - lambdas.reshape(kv_local, group, 1, 1) * second
-    heads_out = (
-        diff * lax.rsqrt(jnp.mean(diff * diff, axis=-1, keepdims=True) + eps) * head_gain
-    ).astype(jnp.bfloat16)
-    weights_out = w_out.reshape(kv_local, group, VDIM, w_out.shape[1])
-    parts = jnp.einsum(
-        "gjrv,gjvd->rd", heads_out, weights_out, preferred_element_type=jnp.float32
-    ).astype(jnp.bfloat16)
-    return run_scatter_sum(n_tp, parts)
+    )(
+        outgoing, kv, queries_a, queries_b, head_gain.reshape(1, -1), lambdas,
+        w_gate, w_up, w_down, w_out,
+    )
 
 
 def fast_body(
     queries_a, queries_b, keys_a, keys_b, values, lambdas, head_gain, w_out,
     moe_tokens, moe_gain, routes, route_weights, w_gate, w_up, w_down,
 ):
-    n, n_tp = lax.axis_size("ep"), lax.axis_size("tp")
+    n = lax.axis_size("ep")
     tok_rows, width = moe_tokens.shape
     cap = 3 * tok_rows * TOP // (2 * n)
     inputs = moe_tokens.astype(jnp.float32)
@@ -517,8 +505,10 @@
         .reshape(n, cap, width)
     )
     kv = jnp.concatenate([keys_a, keys_b, values], axis=1)
-    returned, kv_all = run_exchange(n, outgoing, kv, w_gate[0], w_up[0], w_down[0])
-    mixer_out = attend(queries_a, queries_b, kv_all, lambdas, head_gain, w_out, n_tp)
+    returned, mixer_out = run_exchange(
+        n, outgoing, kv, queries_a, queries_b, head_gain, lambdas,
+        w_gate[0], w_up[0], w_down[0], w_out,
+    )
     slot_ids = routes * cap + jnp.sum(jnp.where(named, place[:, None, :], 0), axis=2)
     table = returned.reshape(n * cap, width)
     total = 0.0
@@ -534,7 +524,7 @@
     n, n_tp = lax.axis_size("ep"), lax.axis_size("tp")
     tok_rows, w_gate = args[8].shape[0], args[12]
     cap = 3 * tok_rows * TOP // (2 * n)
-    if w_gate.shape[0] == 1 and n_tp == 4 and n & (n - 1) == 0 and n >= 4 and cap % 16 == 0:
+    if w_gate.shape[0] == 1 and n_tp == 4 and n & (n - 1) == 0 and n >= 8 and cap % 16 == 0:
         return fast_body(*args)
     return body(*args)
 

time: 154 us -> 123 us (0.80)
  matrix products: 22.7 us -> 6.34 us
  local copies, waits for them, and re-layouts: 10.7 us -> 1.51 us
  Pallas kernels: 112 us -> 108 us
    dot_general x5 -> x0, matrix products: 13.3 us -> none  [the longest x2 8.25 us: one_map(): jnp.einsum('gjrn,ngv->gjrv', expo.astype(jnp.bfloat16), value_rows, prefe...]
    pallas_call x1 -> x0, Pallas kernels: 8.98 us -> none  [run_scatter_sum(): pl.pallas_call(functools.partial(scatter_sum, n), out_shape=jax.ShapeDtyp...]
    pallas_call x1, Pallas kernels: 103 us -> 108 us  [run_exchange(): pl.pallas_call(functools.partial(exchange, n), out_shape=(jax.ShapeDtypeS...]
    unnamed x15 -> x5, local copies, waits for them, and re-layouts: 5.07 us -> 0.66 us
    slice x5 -> x0, local copies, waits for them, and re-layouts: 3.45 us -> none  [the longest x2 2.08 us: attend(): value_rows = kv_rows[:, 2 * span:].reshape(count, kv_local, VDIM)]
    sub x2 -> x0, matrix products: 3.12 us -> none  [one_map(): expo = jnp.where(visible, jnp.exp(scores - peak), 0.0)]
where the time goes in v2:
time: 123 us; the launch traced here: 121 us
  Pallas kernels  108 us (88%)
  matrix products  6.34 us (5%)
  other arithmetic  4.99 us (4%)
  local copies, waits for them, and re-layouts  1.51 us (1%)
    pallas_call x1, Pallas kernels, run_exchange(): pl.pallas_call(functools.partial(exchange, n), out_shape=(jax.ShapeDtypeS...  108 us
    dot_general x2, matrix products, fast_body(): jnp.dot(chosen.astype(jnp.bfloat16), table, preferred_element_type=jnp.fl...  3.3 us
    dot_general x1, matrix products, fast_body(): jnp.dot(pick.astype(jnp.bfloat16), normed, preferred_element_type=jnp.flo...  2.84 us

profile of v2, /device:TPU:0, one launch (start us, length us, event | category | flops | bytes accessed | tf_op | source)
XLA Modules:
  0.0 121.3 jit_solution(889527740287752333)
XLA Ops:
  0.6 1.2 %fusion.2 = f32[128]{0:T(128)S(1)} fusion(bf16[128,2048]{1,0:T(8,128)(2,1)} %param.23), kind=kLoop, calls=%fused_computation.8 | loop fusion | flops 786304 | bytes 524800 | tf_op jit(solution)/shard_map/reduce_sum | solution.py:490
  1.9 0.7 fusion.15
  2.6 0.8 slice_bitcast_fusion.1
  3.3 0.2 convolution_convert_fusion.1
  3.5 0.7 select_reduce_fusion
  4.2 0.7 multiply_add_fusion
  4.9 0.1 eq.69
  5.0 0.1 bitcast_compare_fusion
  5.1 1.5 %pad_maximum_fusion.kv = bf16[128,512]{1,0:T(8,128)(2,1)} fusion(bf16[128,256]{1,0:T(8,128)(2,1)} %param.19, bf16[128,128]{1,0:T(8,128)(2,1)} %param.18, bf16[128,128]{1,0:T(8,128)(2,1)} %param.17), kind=kLoop, calls=%fused_computation.16 | loop fusion | flops 393216 | bytes 262144 | tf_op jit(solution)/shard_map/concatenate | solution.py:507
  6.7 2.8 %convolution_convert_fusion = bf16[384,2048]{1,0:T(8,128)(2,1)} fusion(pred[384,128]{1,0:T(32,128)(4,1)S(1)} %bitcast_compare_fusion, bf16[128,2048]{1,0:T(8,128)(2,1)} %param.23, f32[2048]{0:T(1024)} %param.24, f32[128]{0:T(128)S(1)} %add_rsqrt_fusion), kind=kOutput, calls=%fused_computation | convolution fusion | flops 203161600 | bytes 2155008 | tf_op jit(solution)/shard_map/dot_general | solution.py:503
  9.5 107.8 %exchange.1 = (bf16[8,48,2048]{2,1,0:T(8,128)(2,1)}, bf16[32,2048]{1,0:T(8,128)(2,1)}) custom-call(bf16[8,48,2048]{2,1,0:T(8,128)(2,1)} %bitcast.24, bf16[128,512]{1,0:T(8,128)(2,1)} %pad_maximum_fusion.kv, bf16[128,256]{1,0:T(8,128)(2,1)} %queries_a.1, bf16[128,256]{1,0:T(8,128)(2,1)} %queries_b.1, f32[1,128]{1,0:T(1,128)} %bitcast.28, f32[4]{0:T(128)} %lambdas.1, ...), custom_call_target="tpu_custom_call" | custom-call | tf_op jit(solution)/shard_map/exchange/pallas_call | solution.py:442
  117.4 0.0 copy-start
  117.4 2.0 %convolution_multiply_fusion.1 = f32[128,2048]{1,0:T(8,128)S(1)} fusion(bf16[384,2048]{1,0:T(8,128)(2,1)} %bitcast.22, f32[128]{0:T(128)S(1)} %get-tuple-element.9, s32[128]{0:T(128)S(1)} %get-tuple-element.7), kind=kOutput, calls=%fused_computation.3 | convolution fusion | flops 201637888 | bytes 2622464 | tf_op jit(solution)/shard_map/dot_general | solution.py:517
  119.4 0.0 copy-done
  119.4 0.0 copy-start.1
  119.4 1.3 %fusion.1 = bf16[128,2048]{1,0:T(8,128)(2,1)} fusion(f32[128,2048]{1,0:T(8,128)S(1)} %convolution_multiply_fusion.1, bf16[384,2048]{1,0:T(8,128)(2,1)S(1)} %bitcast.23, f32[128]{0:T(128)S(1)} %get-tuple-element.8, s32[128]{0:T(128)S(1)} %get-tuple-element.6), kind=kOutput, calls=%fused_computation.4 | convolution fusion | flops 202162176 | bytes 3146752 | tf_op jit(solution)/shard_map/dot_general | solution.py:517
  120.7 0.0 copy-done.1
  120.7 0.7 copy.22
  (5 shorter events, 0.0 us)
Async XLA Ops:
  117.4 2.0 %copy-start = (bf16[8,48,2048]{2,1,0:T(8,128)(2,1)S(1)}, bf16[8,48,2048]{2,1,0:T(8,128)(2,1)}, u32[]{:S(2)}) copy-start(bf16[8,48,2048]{2,1,0:T(8,128)(2,1)} %get-tuple-element.5) | copy-start | bytes 4718596
  119.4 1.3 %copy-start.1 = (bf16[32,2048]{1,0:T(8,128)(2,1)S(1)}, bf16[32,2048]{1,0:T(8,128)(2,1)}, u32[]{:S(2)}) copy-start(bf16[32,2048]{1,0:T(8,128)(2,1)} %get-tuple-element.12) | copy-start | bytes 393220
